TPU v7x, 32 devices: a whole 2x2x4 slice. The times are simulated.
32 devices in a mesh: sp: 16 (over z, y, x), tp: 2 (over core).
Axes of the slice: x: 2, y: 2, z: 4, core: 2. Of those that a mesh axis runs over, the one named last changes fastest.
Arguments:
- residual: bfloat16 [4096, 2048], P(('sp', 'tp')), may hold values from -6 to 6
- pool_input: bfloat16 [4096, 1024], P('sp', 'tp'), may hold values from -6 to 6
- group_maps: bfloat16 [8, 128, 128], replicated, may hold values from -0.5 to 0.5
- pool_scale: float32 [1024], replicated, may hold values from 0.1 to 1.9
- out_proj: bfloat16 [1024, 2048], replicated, may hold values from -0.1875 to 0.1875
- norm_gain: float32 [2048], replicated, may hold values from 0.1 to 1.9
- shared_gate: bfloat16 [2048, 512], replicated, may hold values from -0.125 to 0.125
- shared_up: bfloat16 [2048, 512], replicated, may hold values from -0.125 to 0.125
- shared_down: bfloat16 [512, 2048], replicated, may hold values from -0.25 to 0.25
- expert_gate: bfloat16 [32, 2048, 512], P(('sp', 'tp')), may hold values from -0.125 to 0.125
- expert_up: bfloat16 [32, 2048, 512], P(('sp', 'tp')), may hold values from -0.125 to 0.125
- expert_down: bfloat16 [32, 512, 2048], P(('sp', 'tp')), may hold values from -0.25 to 0.25
- expert_ids: int32 [4096, 4], P(('sp', 'tp')), may hold values from 0 to 31, all different within a row; in each aligned block of 128 rows (0 to 127, 128 to 255, ...) at most 24 rows name the same one
- route_score: float32 [4096, 4], P(('sp', 'tp')), may hold values from 0.05 to 1
Outputs:
- output: bfloat16 [4096, 2048], P(('sp', 'tp'))
Inputs may be any that keep to these rules, and one draw needn't show every extreme that they name: `expert_ids`: each row names 4 different experts; among the 128 rows of one device no expert is named more than 24 times, and in some devices' rows one expert is named exactly 24 times.
All inputs are finite; a program needn't handle non-finite values.
Results may differ from a plain program's by a relative error of at most 0.015.
Values may be sent and summed in bfloat16 or wider, within the bound.
A program may use at most 128 MiB of HBM per device.

v0:
```python
import jax
import jax.numpy as jnp
from jax import lax
from jax.sharding import PartitionSpec as P

windows = (2, 4, 8, 16)
epsilon = 1e-06
routed_scale = 2.5


def from_behind(shard, axis, by):
    peers = lax.axis_size(axis)
    pairs = [(i, i + by) for i in range(peers) if 0 <= i + by < peers]
    return lax.ppermute(shard, axis, pairs)


def swiglu(row_block, w_gate, w_up, w_down):
    gate_part = jnp.dot(row_block, w_gate, preferred_element_type=jnp.float32)
    up_part = jnp.dot(row_block, w_up, preferred_element_type=jnp.float32)
    hidden = (jax.nn.silu(gate_part) * up_part).astype(jnp.bfloat16)
    return jnp.dot(hidden, w_down, preferred_element_type=jnp.float32)


def on_device(
    residual,
    pool_input,
    group_maps,
    pool_scale,
    out_proj,
    norm_gain,
    shared_gate,
    shared_up,
    shared_down,
    expert_gate,
    expert_up,
    expert_down,
    expert_ids,
    route_score,
):
    row_count, channels = pool_input.shape
    group_width = group_maps.shape[1]
    groups_here = channels // group_width
    halo_reach = max(windows) - 1
    before = from_behind(pool_input[row_count - halo_reach :], "sp", 1)
    extended = (
        jnp.concatenate([before, pool_input], axis=0)
        .astype(jnp.float32)
        .reshape(row_count + halo_reach, groups_here, group_width)
    )
    places = lax.axis_index("sp") * row_count + jnp.arange(row_count, dtype=jnp.int32)
    pooled = []
    for group_index in range(groups_here):
        running_sum = extended[:, group_index]
        window_span = 1
        while window_span < windows[group_index % 4]:
            running_sum = running_sum[window_span:] + running_sum[:-window_span]
            window_span = window_span * 2
        divisor = jnp.minimum(places + 1, window_span).astype(jnp.float32)[:, None]
        pooled.append(running_sum[running_sum.shape[0] - row_count :] / divisor)
    pooled = jnp.stack(pooled, axis=1)
    contrast = (pooled - extended[halo_reach:]).astype(jnp.bfloat16)
    first_group = lax.axis_index("tp") * groups_here
    maps_here = lax.dynamic_slice_in_dim(group_maps, first_group, groups_here, 0)
    mapped = jnp.einsum("sgc,gcd->sgd", contrast, maps_here, preferred_element_type=jnp.float32)
    scale_here = lax.dynamic_slice_in_dim(pool_scale, first_group * group_width, channels, 0)
    mixed_rows = (mapped.reshape(row_count, channels) * scale_here).astype(jnp.bfloat16)
    model_width = out_proj.shape[1]
    swapped = lax.all_to_all(mixed_rows, "tp", split_axis=0, concat_axis=1, tiled=True)
    projected = jnp.dot(swapped, out_proj, preferred_element_type=jnp.float32)
    settled = (residual.astype(jnp.float32) + projected).astype(jnp.bfloat16)
    settled_wide = settled.astype(jnp.float32)
    inverse_rms = lax.rsqrt(jnp.mean(settled_wide * settled_wide, axis=-1, keepdims=True) + epsilon)
    normed = (settled_wide * inverse_rms * norm_gain).astype(jnp.bfloat16)
    shared = swiglu(normed, shared_gate, shared_up, shared_down)
    tokens_here, top_count = expert_ids.shape
    size_sp = lax.axis_size("sp")
    size_tp = lax.axis_size("tp")
    experts = size_sp * size_tp
    capacity = 3 * tokens_here * top_count // (2 * experts)
    assigned = tokens_here * top_count
    flat_ids = expert_ids.reshape(assigned)
    onehot = (flat_ids[:, None] == jnp.arange(experts, dtype=jnp.int32)[None, :]).astype(
        jnp.bfloat16
    )
    earlier = (jnp.arange(assigned)[None, :] < jnp.arange(assigned)[:, None]).astype(jnp.bfloat16)
    before_counts = jnp.dot(earlier, onehot, preferred_element_type=jnp.float32)
    position = jnp.sum(before_counts * onehot, axis=1).astype(jnp.int32)
    slot_index = position * experts + flat_ids
    slot_token = (
        jnp.zeros((capacity * experts,), jnp.int32)
        .at[slot_index]
        .set(jnp.arange(assigned, dtype=jnp.int32) // top_count)
    )
    outgoing = normed[slot_token].reshape(capacity, experts, model_width)
    arrived = lax.all_to_all(outgoing, ("sp", "tp"), split_axis=1, concat_axis=1, tiled=True)
    item_total = arrived.shape[0]
    flat_rows = arrived.reshape(item_total * experts, model_width)
    expert_rows = swiglu(flat_rows, expert_gate[0], expert_up[0], expert_down[0]).astype(
        jnp.bfloat16
    )
    results = expert_rows.reshape(item_total, experts, model_width)
    returned = lax.all_to_all(results, ("sp", "tp"), split_axis=1, concat_axis=1, tiled=True)
    picked = returned.reshape(capacity * experts, model_width)[slot_index].reshape(
        tokens_here, top_count, model_width
    )
    weights = route_score / jnp.sum(route_score, axis=-1, keepdims=True) * routed_scale
    routed = jnp.einsum("tk,tkd->td", weights, picked.astype(jnp.float32))
    return (settled_wide + shared + routed).astype(jnp.bfloat16)


def solution(mesh):
    in_specs = (
        P(("sp", "tp"), None),
        P("sp", "tp"),
        P(),
        P(),
        P(),
        P(),
        P(),
        P(),
        P(),
        P(("sp", "tp"), None, None),
        P(("sp", "tp"), None, None),
        P(("sp", "tp"), None, None),
        P(("sp", "tp"), None),
        P(("sp", "tp"), None),
    )
    out_specs = P(("sp", "tp"), None)
    return jax.shard_map(
        on_device, mesh=mesh, in_specs=in_specs, out_specs=out_specs, check_vma=False
    )
```

profile of v0, /device:TPU:0, one launch (start us, length us, event | category | flops | bytes accessed | tf_op | source)
XLA Modules:
  0.0 225.8 jit_solution(15422109679087078198)
XLA Ops:
  0.0 0.0 copy-start
  0.0 0.9 slice.118
  0.9 4.9 %collective-permute-start = (bf16[15,512]{1,0:T(8,128)(2,1)S(1)}, bf16[15,512]{1,0:T(8,128)(2,1)S(1)}, u32[]{:S(2)}, u32[]{:S(2)}) collective-permute-start(bf16[15,512]{1,0:T(8,128)(2,1)S(1)} %slice.118), channel_id=1, source_target_pairs={{0,2},{2,4},{4,6},{6,8},{8,10},{10,12},{12,14},{14,16},{16,18},{18... | collective-permute-start | bytes 46088 | tf_op jit(solution)/shard_map/ppermute | solution.py:14
  5.7 1.0 copy_bitcast_fusion
  6.7 0.8 copy.41
  7.5 0.1 eq.15
  7.6 0.1 reshape.132
  7.8 0.3 fusion.12
  8.1 2.4 %scatter_custom_fusion = s32[768]{0:T(1024)S(1)} fusion(s32[512]{0:T(512)S(1)} %bitcast.90, s32[512]{0:T(512)S(1)} %add_select_fusion, s32[]{:T(128)} %constant.23.clone.1), kind=kCustom, calls=%fused_computation.73 | custom fusion | bytes 3076 | tf_op jit(solution)/shard_map/scatter | solution.py:92
  10.6 0.8 dynamic_slice.7
  11.4 0.0 collective-permute-done
  11.4 0.1 maximum_convert_fusion
  11.5 0.1 fusion.48
  11.5 0.0 copy-start.3
  11.5 0.0 copy-start.4
  11.7 0.1 fusion.25
  11.8 0.1 fusion.28
  11.9 0.1 fusion.31
  12.0 0.1 fusion.34
  12.1 0.3 copy-done.3
  12.5 0.1 copy-done.4
  12.6 0.3 convolution_bitcast_fusion
  12.8 0.3 reshape.131
  13.1 0.1 fusion.16
  13.3 3.9 %all_to_all.26 = bf16[2,128,512]{1,2,0:T(8,128)(2,1)S(1)} all-to-all(bf16[2,128,512]{1,2,0:T(8,128)(2,1)S(1)} %fusion.16), channel_id=1, replica_groups=mesh['sp'=16,'tp'=2] {'tp'}, dimensions={0} | all-to-all | bytes 524288 | tf_op jit(solution)/shard_map/all_to_all | solution.py:68
  17.2 3.1 %multiply_reduce_fusion = (f32[128]{0:T(128)S(1)}, f32[128,2048]{1,0:T(8,128)S(1)}) fusion(bf16[128,1024]{0,1:T(8,128)(2,1)S(1)} %bitcast.89, bf16[1024,2048]{1,0:T(8,128)(2,1)} %param.18, bf16[128,2048]{1,0:T(8,128)(2,1)} %param.14), kind=kOutput, calls=%fused_computation.23 | convolution fusion | flops 538443648 | bytes 6029824 | tf_op jit(solution)/shard_map/dot_general | solution.py:69
  20.3 0.0 copy-start.1
  20.4 1.1 copy-done.1
  21.4 0.0 copy-done.5
  21.4 0.2 multiply_convert_fusion.1
  21.6 4.2 %gather_fusion = bf16[768,2048]{1,0:T(8,128)(2,1)} fusion(bf16[128,2048]{1,0:T(8,128)(2,1)S(1)} %multiply_convert_fusion.1, s32[1024]{0:T(1024)S(1)} %pad_clamp_fusion.1), kind=kCustom, calls=%fused_computation | custom fusion | bytes 6294528 | tf_op jit(solution)/shard_map/gather | solution.py:94
  25.8 3.6 %copy.43 = bf16[24,32,2048]{2,0,1:T(8,128)(2,1)S(1)} copy(bf16[24,32,2048]{2,1,0:T(8,128)(2,1)} %bitcast.85) | data formatting | bytes 6291456 | tf_op jit(solution)/shard_map/reshape | solution.py:94
  29.5 75.9 %all_to_all.27 = bf16[24,32,2048]{2,0,1:T(8,128)(2,1)S(1)} all-to-all(bf16[24,32,2048]{2,0,1:T(8,128)(2,1)S(1)} %copy.43), channel_id=1, replica_groups=mesh['sp'=16,'tp'=2] {'sp','tp'}, dimensions={1} | all-to-all | bytes 6291456 | tf_op jit(solution)/shard_map/all_to_all | solution.py:95
  105.3 1.7 copy.44
  107.1 0.0 copy-start.2
  107.1 1.7 copy-done.2
  108.7 2.9 %fusion.7 = f32[768,512]{1,0:T(8,128)} fusion(bf16[768,2048]{1,0:T(8,128)(2,1)S(1)} %bitcast.86, bf16[1,2048,512]{2,1,0:T(8,128)(2,1)S(1)} %copy-done.7), kind=kOutput, calls=%fused_computation.13 | convolution fusion | flops 1610612736 | bytes 6815744 | tf_op jit(solution)/shard_map/dot_general | solution.py:18
  111.7 8.1 %convolution_convert_fusion = bf16[768,2048]{1,0:T(8,128)(2,1)} fusion(bf16[1,512,2048]{2,1,0:T(8,128)(2,1)S(1)} %copy-done, f32[768,512]{1,0:T(8,128)} %fusion.7, bf16[768,2048]{1,0:T(8,128)(2,1)} %bitcast.87, bf16[1,2048,512]{2,1,0:T(8,128)(2,1)} %param.24), kind=kOutput, calls=%fused_computation.3 | convolution fusion | flops 3225157632 | bytes 12058624 | tf_op jit(solution)/shard_map/dot_general | solution.py:21
  119.8 5.3 %copy.45 = bf16[24,32,2048]{2,0,1:T(8,128)(2,1)} copy(bf16[24,32,2048]{2,1,0:T(8,128)(2,1)} %bitcast.88) | data formatting | bytes 6291456 | tf_op jit(solution)/shard_map/reshape | solution.py:101
  125.1 4.0 %all-to-all-start.2 = ((bf16[24,32,2048]{2,0,1:T(8,128)(2,1)}), bf16[24,32,2048]{2,0,1:T(8,128)(2,1)}, u32[]{:S(2)}, u32[]{:S(2)}) async-start(bf16[24,32,2048]{2,0,1:T(8,128)(2,1)} %copy.45), calls=%async_computation.2 | async-start | bytes 6291456 | tf_op jit(solution)/shard_map/all_to_all | solution.py:102
  129.1 0.1 copy.47
  129.3 2.0 fusion.51
  131.4 69.0 %all-to-all-done.2 = bf16[24,32,2048]{2,0,1:T(8,128)(2,1)} async-done(((bf16[24,32,2048]{2,0,1:T(8,128)(2,1)}), bf16[24,32,2048]{2,0,1:T(8,128)(2,1)}, u32[]{:S(2)}, u32[]{:S(2)}) %all-to-all-start.2) | async-done | bytes 3145760 | tf_op jit(solution)/shard_map/all_to_all | solution.py:102
  200.3 5.3 %copy.46 = bf16[24,32,2048]{2,1,0:T(8,128)(2,1)} copy(bf16[24,32,2048]{2,0,1:T(8,128)(2,1)} %all-to-all-done.2) | data formatting | bytes 6291456 | tf_op jit(solution)/shard_map/all_to_all | solution.py:102
  205.6 7.6 %gather_fusion.1 = bf16[512,2048]{1,0:T(8,128)(2,1)} fusion(bf16[768,2048]{1,0:T(8,128)(2,1)} %bitcast.84, s32[1024]{0:T(1024)S(1)} %pad_clamp_fusion), kind=kCustom, calls=%fused_computation.1 | custom fusion | bytes 4196352 | tf_op jit(solution)/shard_map/gather | solution.py:103
  213.2 4.1 %reshape.137 = bf16[128,4,2048]{2,1,0:T(4,128)(2,1)} reshape(bf16[512,2048]{1,0:T(8,128)(2,1)} %gather_fusion.1) | data formatting | bytes 4194304 | tf_op jit(solution)/shard_map/reshape | solution.py:103
  217.3 3.8 %fusion.52 = f32[128,1,2048]{2,1,0:T(1,128)} fusion(bf16[128,4,1]{1,2,0:T(2,128)(2,1)S(1)} %copy.47, bf16[128,4,2048]{2,1,0:T(4,128)(2,1)} %reshape.137), kind=kOutput, calls=%fused_computation.91 | convolution fusion | flops 2097152 | bytes 3146752 | tf_op jit(solution)/shard_map/tk,tkd->td/dot_general | solution.py:107
  221.1 4.7 %fusion.3 = bf16[128,2048]{1,0:T(8,128)(2,1)} fusion(f32[128,2048]{1,0:T(8,128)} %copy-done.1, bf16[512,2048]{1,0:T(8,128)(2,1)} %param.22, bf16[128,2048]{1,0:T(8,128)(2,1)S(1)} %multiply_convert_fusion.1, bf16[2048,512]{1,0:T(8,128)(2,1)} %param.21, f32[128,1,2048]{2,1,0:T(1,128)} %fusion.52, f32[128,512]{1,0:T(8,128)S(1)} %fusion.51), kind=kOutput, calls=%fused_computation.9 | convolution fusion | flops 538050560 | bytes 7602176 | tf_op jit(solution)/shard_map/dot_general | solution.py:21
  (23 shorter events, 0.2 us)
Async XLA Ops:
  0.0 111.7 %copy-start = (bf16[1,512,2048]{2,1,0:T(8,128)(2,1)S(1)}, bf16[1,512,2048]{2,1,0:T(8,128)(2,1)}, u32[]{:S(2)}) copy-start(bf16[1,512,2048]{2,1,0:T(8,128)(2,1)} %param.25) | copy-start | bytes 6291460
  0.9 10.5 %collective-permute-start = (bf16[15,512]{1,0:T(8,128)(2,1)S(1)}, bf16[15,512]{1,0:T(8,128)(2,1)S(1)}, u32[]{:S(2)}, u32[]{:S(2)}) collective-permute-start(bf16[15,512]{1,0:T(8,128)(2,1)S(1)} %slice.118), channel_id=1, source_target_pairs={{0,2},{2,4},{4,6},{6,8},{8,10},{10,12},{12,14},{14,16},{16,18},{18... | collective-permute-start | bytes 46088 | tf_op jit(solution)/shard_map/ppermute | solution.py:14
  11.5 1.0 copy-start.3
  11.5 1.0 copy-start.4
  17.2 4.2 %copy-start.5 = (f32[2048]{0:T(1024)S(1)}, f32[2048]{0:T(1024)}, u32[]{:S(2)}) copy-start(f32[2048]{0:T(1024)} %param.19) | copy-start | bytes 24580
  20.3 1.1 copy-start.1
  105.3 3.4 %copy-start.7 = (bf16[1,2048,512]{2,1,0:T(8,128)(2,1)S(1)}, bf16[1,2048,512]{2,1,0:T(8,128)(2,1)}, u32[]{:S(2)}) copy-start(bf16[1,2048,512]{2,1,0:T(8,128)(2,1)} %param.23) | copy-start | bytes 6291460
  107.1 1.7 copy-start.2
  125.1 4.0 %copy-start.6 = (f32[128,4]{0,1:T(4,128)S(1)}, f32[128,4]{0,1:T(4,128)}, u32[]{:S(2)}) copy-start(f32[128,4]{0,1:T(4,128)} %param.27) | copy-start | bytes 6148
  125.1 75.3 %all-to-all-start.2 = ((bf16[24,32,2048]{2,0,1:T(8,128)(2,1)}), bf16[24,32,2048]{2,0,1:T(8,128)(2,1)}, u32[]{:S(2)}, u32[]{:S(2)}) async-start(bf16[24,32,2048]{2,0,1:T(8,128)(2,1)} %copy.45), calls=%async_computation.2 | async-start | bytes 6291456 | tf_op jit(solution)/shard_map/all_to_all | solution.py:102
where the time goes:
time: 226 us
  blocking collectives  79.8 us (35%)
  waiting for transfers between devices  69 us (31%)
  local copies, waits for them, and re-layouts  41.6 us (18%)
  matrix products  25.2 us (11%)
  starting transfers between devices  8.87 us (4%)
    all_to_all x1, blocking collectives, on_device(): lax.all_to_all(outgoing, ('sp', 'tp'), split_axis=1, concat_axis=1, tiled...  75.9 us
    all_to_all x1, waiting for transfers between devices, on_device(): lax.all_to_all(results, ('sp', 'tp'), split_axis=1, concat_axis=1, tiled=...  69 us
    dot_general x2, matrix products, swiglu(): return jnp.dot(hidden, w_down, preferred_element_type=jnp.float32)  12.8 us
    gather x1, local copies, waits for them, and re-layouts, on_device(): returned.reshape(capacity * experts, model_width)[slot_index]  7.58 us
    all_to_all x1, local copies, waits for them, and re-layouts, on_device(): lax.all_to_all(results, ('sp', 'tp'), split_axis=1, concat_axis=1, tiled=...  5.29 us
    reshape x1, local copies, waits for them, and re-layouts, on_device(): results = expert_rows.reshape(item_total, experts, model_width)  5.29 us
    dot_general x2, matrix products, swiglu(): gate_part = jnp.dot(row_block, w_gate, preferred_element_type=jnp.float32)  4.97 us
    ppermute x1, starting transfers between devices, from_behind(): return lax.ppermute(shard, axis, pairs)  4.86 us
  transfers between devices with their start and end apart: 2, of which 1 were waited for; matrix products, arithmetic and copies ran while one was open for 3% of the time, Pallas kernels for 0%

commit v1 on v0

--- a/solution.py
+++ b/solution.py
@@ -1,6 +1,11 @@
+import functools
+import math
+
 import jax
 import jax.numpy as jnp
 from jax import lax
+from jax.experimental import pallas as pl
+from jax.experimental.pallas import tpu as pltpu
 from jax.sharding import PartitionSpec as P
 
 windows = (2, 4, 8, 16)
@@ -14,11 +19,315 @@
     return lax.ppermute(shard, axis, pairs)
 
 
-def swiglu(row_block, w_gate, w_up, w_down):
-    gate_part = jnp.dot(row_block, w_gate, preferred_element_type=jnp.float32)
-    up_part = jnp.dot(row_block, w_up, preferred_element_type=jnp.float32)
-    hidden = (jax.nn.silu(gate_part) * up_part).astype(jnp.bfloat16)
-    return jnp.dot(hidden, w_down, preferred_element_type=jnp.float32)
+def layer_count(size_sp):
+    return max(d for d in range(1, math.isqrt(size_sp) + 1) if size_sp % d == 0)
+
+
+def moe_kernel(
+    layers,
+    peers,
+    cores,
+    cap,
+    top,
+    normed_ref,
+    settled_ref,
+    meta_ref,
+    sg_hbm,
+    su_hbm,
+    sd_hbm,
+    eg_hbm,
+    eu_hbm,
+    ed_hbm,
+    out_ref,
+    gathered,
+    metas,
+    packed,
+    arrived,
+    results,
+    back,
+    part,
+    landed,
+    acc,
+    sg,
+    su,
+    sd,
+    eg,
+    eu,
+    ed,
+    w_sem,
+    own_sem,
+    z_send,
+    z_recv,
+    m_send,
+    m_recv,
+    a_send,
+    a_recv,
+    b_send,
+    b_recv,
+    c_send,
+    c_recv,
+):
+    per_layer = peers // cores
+    sp = lax.axis_index("sp")
+    core = lax.axis_index("tp")
+    z = sp // per_layer
+    q = sp % per_layer
+    me = q * cores + core
+    tokens, width = normed_ref.shape
+    slots = peers * cap
+    step_cols = min(width, 512)
+
+    def in_column(s):
+        return (s * per_layer + q, core)
+
+    def in_layer(p):
+        return (z * per_layer + p // cores, p % cores)
+
+    def remote(src, dst, send, recv, to):
+        return pltpu.make_async_remote_copy(
+            src_ref=src,
+            dst_ref=dst,
+            send_sem=send,
+            recv_sem=recv,
+            device_id=to,
+            device_id_type=pl.DeviceIdType.MESH,
+        )
+
+    loads = [
+        pltpu.make_async_copy(a, b, w_sem.at[i])
+        for i, (a, b) in enumerate(
+            (
+                (sg_hbm, sg),
+                (su_hbm, su),
+                (sd_hbm, sd),
+                (eg_hbm.at[0], eg),
+                (eu_hbm.at[0], eu),
+                (ed_hbm.at[0], ed),
+            )
+        )
+    ]
+    own_rows = pltpu.make_async_copy(normed_ref, gathered.at[z], own_sem.at[0])
+    own_meta = pltpu.make_async_copy(meta_ref, metas.at[z], own_sem.at[1])
+    own_rows.start()
+    own_meta.start()
+
+    barrier = pltpu.get_barrier_semaphore()
+    for o in range(1, layers):
+        pl.semaphore_signal(
+            barrier, inc=1, device_id=in_column((z + o) % layers),
+            device_id_type=pl.DeviceIdType.MESH,
+        )
+    for o in range(1, peers):
+        pl.semaphore_signal(
+            barrier, inc=1, device_id=in_layer((me + o) % peers),
+            device_id_type=pl.DeviceIdType.MESH,
+        )
+    pl.semaphore_wait(barrier, layers - 1 + peers - 1)
+    own_rows.wait()
+    own_meta.wait()
+
+    def meta_copy(target, source):
+        return remote(
+            metas.at[source], metas.at[source], m_send.at[target], m_recv.at[source],
+            in_column(target),
+        )
+
+    for o in range(1, layers):
+        meta_copy((z + o) % layers, z).start()
+
+    def chunk_copy(s, side):
+        to = z + 1 if side == 0 else z - 1
+        to = jnp.clip(to, 0, layers - 1)
+        return remote(
+            gathered.at[s], gathered.at[s], z_send.at[side, s], z_recv.at[s], in_column(to)
+        )
+
+    def goes_up(s):
+        return jnp.logical_and(s <= z, z < layers - 1)
+
+    def goes_down(s):
+        return jnp.logical_and(s >= z, z > 0)
+
+    def pack_copy(s, p, source):
+        return remote(
+            packed.at[s, p], arrived.at[s, source], a_send.at[s, p], a_recv.at[s, source],
+            in_layer(p),
+        )
+
+    def back_copy(s, p, source):
+        return remote(
+            results.at[s, p], back.at[s, source], b_send.at[s, p], b_recv.at[s, source],
+            in_layer(p),
+        )
+
+    def part_copy(s, source):
+        return remote(
+            part.at[s], landed.at[source], c_send.at[s], c_recv.at[source], in_column(s)
+        )
+
+    def own_pack(s):
+        return pltpu.make_async_copy(packed.at[s, me], arrived.at[s, me], a_recv.at[s, me])
+
+    def own_back(s):
+        return pltpu.make_async_copy(results.at[s, me], back.at[s, me], b_recv.at[s, me])
+
+    near = jnp.minimum(z, layers - 1 - z)
+
+    def chunk_at(i):
+        both = (i + 1) // 2
+        two_sided = jnp.where(i % 2 == 1, z - both, z + both)
+        one_sided = jnp.where(2 * z <= layers - 1, z + (i - near), z - (i - near))
+        return jnp.where(i <= 2 * near, two_sided, one_sided)
+
+    def slot_table(s, value):
+        ids = lax.broadcasted_iota(jnp.int32, (slots, tokens), 0).astype(jnp.float32)
+        ids = ids + (z * slots).astype(jnp.float32)
+        table = jnp.zeros((slots, tokens), jnp.float32)
+        rows = metas[s]
+        for k in range(top):
+            hit = ids == rows[k : k + 1]
+            table = table + jnp.where(hit, rows[top + k : top + k + 1] if value else 1.0, 0.0)
+        return table
+
+    def dispatch(i):
+        s = chunk_at(i)
+
+        @pl.when(i > 0)
+        def _():
+            chunk_copy(s, 0).wait_recv()
+
+        @pl.when(goes_up(s))
+        def _():
+            chunk_copy(s, 0).start()
+
+        @pl.when(goes_down(s))
+        def _():
+            chunk_copy(s, 1).start()
+
+        @pl.when(i > 0)
+        def _():
+            meta_copy(z, s).wait_recv()
+
+        table = slot_table(s, False).astype(jnp.bfloat16)
+        for col in range(0, width, step_cols):
+            got = jnp.dot(
+                table, gathered[s, :, col : col + step_cols], preferred_element_type=jnp.float32
+            )
+            packed[s, :, :, col : col + step_cols] = (
+                got.astype(jnp.bfloat16).reshape(peers, cap, step_cols)
+            )
+        for o in range(1, peers):
+            pack_copy(s, (me + o) % peers, me).start()
+        own_pack(s).start()
+
+    def mlp(rows, w_gate, w_up):
+        gate = jnp.dot(rows, w_gate[...], preferred_element_type=jnp.float32)
+        up = jnp.dot(rows, w_up[...], preferred_element_type=jnp.float32)
+        return (gate / (1.0 + jnp.exp(-gate)) * up).astype(jnp.bfloat16)
+
+    def expert(i):
+        s = chunk_at(i)
+        for o in range(1, peers):
+            p = (me + o) % peers
+            pack_copy(s, p, p).wait_recv()
+        own_pack(s).wait()
+        hidden = mlp(arrived[s].reshape(slots, width), eg, eu)
+        for col in range(0, width, step_cols):
+            got = jnp.dot(hidden, ed[:, col : col + step_cols], preferred_element_type=jnp.float32)
+            results[s, :, :, col : col + step_cols] = (
+                got.astype(jnp.bfloat16).reshape(peers, cap, step_cols)
+            )
+        for o in range(1, peers):
+            back_copy(s, (me + o) % peers, me).start()
+        own_back(s).start()
+
+    def combine(i):
+        s = chunk_at(i)
+        for o in range(1, peers):
+            p = (me + o) % peers
+            back_copy(s, p, p).wait_recv()
+        own_back(s).wait()
+        table = slot_table(s, True)
+        high = table.astype(jnp.bfloat16)
+        low = (table - high.astype(jnp.float32)).astype(jnp.bfloat16)
+        dims = (((0,), (0,)), ((), ()))
+        for col in range(0, width, step_cols):
+            rows = back[s, :, :, col : col + step_cols].reshape(slots, step_cols)
+            got = lax.dot_general(high, rows, dims, preferred_element_type=jnp.float32)
+            got = got + lax.dot_general(low, rows, dims, preferred_element_type=jnp.float32)
+
+            @pl.when(i == 0)
+            def _():
+                acc[:, col : col + step_cols] = acc[:, col : col + step_cols] + got
+
+            @pl.when(i > 0)
+            def _():
+                part[s, :, col : col + step_cols] = got.astype(jnp.bfloat16)
+
+        @pl.when(i > 0)
+        def _():
+            part_copy(s, z).start()
+
+    def shared():
+        for load in loads:
+            load.wait()
+        hidden = mlp(normed_ref[...], sg, su)
+        for col in range(0, width, step_cols):
+            got = jnp.dot(hidden, sd[:, col : col + step_cols], preferred_element_type=jnp.float32)
+            acc[:, col : col + step_cols] = got + settled_ref[:, col : col + step_cols].astype(
+                jnp.float32
+            )
+
+    def step(i, carry):
+        @pl.when(i < layers)
+        def _():
+            dispatch(i)
+
+        @pl.when(i == 0)
+        def _():
+            shared()
+
+        @pl.when(jnp.logical_and(i >= 1, i <= layers))
+        def _():
+            expert(i - 1)
+
+        @pl.when(i >= 2)
+        def _():
+            combine(i - 2)
+
+        return carry
+
+    for load in loads:
+        load.start()
+    lax.fori_loop(0, layers + 2, step, 0)
+
+    def drain(s, carry):
+        @pl.when(goes_up(s))
+        def _():
+            chunk_copy(s, 0).wait_send()
+
+        @pl.when(goes_down(s))
+        def _():
+            chunk_copy(s, 1).wait_send()
+
+        for o in range(1, peers):
+            p = (me + o) % peers
+            pack_copy(s, p, me).wait_send()
+            back_copy(s, p, me).wait_send()
+        return carry
+
+    lax.fori_loop(0, layers, drain, 0)
+    for o in range(1, layers):
+        s = (z + o) % layers
+        meta_copy(s, z).wait_send()
+        part_copy(s, z).wait_send()
+        part_copy(s, s).wait_recv()
+    for col in range(0, width, step_cols):
+        total = acc[:, col : col + step_cols]
+        for o in range(1, layers):
+            s = (z + o) % layers
+            total = total + landed[s, :, col : col + step_cols].astype(jnp.float32)
+        out_ref[:, col : col + step_cols] = total.astype(jnp.bfloat16)
 
 
 def on_device(
@@ -71,12 +380,14 @@
     settled_wide = settled.astype(jnp.float32)
     inverse_rms = lax.rsqrt(jnp.mean(settled_wide * settled_wide, axis=-1, keepdims=True) + epsilon)
     normed = (settled_wide * inverse_rms * norm_gain).astype(jnp.bfloat16)
-    shared = swiglu(normed, shared_gate, shared_up, shared_down)
     tokens_here, top_count = expert_ids.shape
     size_sp = lax.axis_size("sp")
     size_tp = lax.axis_size("tp")
     experts = size_sp * size_tp
     capacity = 3 * tokens_here * top_count // (2 * experts)
+    cap = -(-capacity // 8) * 8
+    layers = layer_count(size_sp)
+    peers = experts // layers
     assigned = tokens_here * top_count
     flat_ids = expert_ids.reshape(assigned)
     onehot = (flat_ids[:, None] == jnp.arange(experts, dtype=jnp.int32)[None, :]).astype(
@@ -84,28 +395,66 @@
     )
     earlier = (jnp.arange(assigned)[None, :] < jnp.arange(assigned)[:, None]).astype(jnp.bfloat16)
     before_counts = jnp.dot(earlier, onehot, preferred_element_type=jnp.float32)
-    position = jnp.sum(before_counts * onehot, axis=1).astype(jnp.int32)
-    slot_index = position * experts + flat_ids
-    slot_token = (
-        jnp.zeros((capacity * experts,), jnp.int32)
-        .at[slot_index]
-        .set(jnp.arange(assigned, dtype=jnp.int32) // top_count)
+    position = jnp.sum(before_counts * onehot, axis=1)
+    slot = (flat_ids.astype(jnp.float32) * cap + position).reshape(tokens_here, top_count)
+    weights = route_score / jnp.sum(route_score, axis=-1, keepdims=True) * routed_scale
+    meta = jnp.concatenate([slot, weights], axis=1).T
+    hidden_width = shared_gate.shape[1]
+    expert_width = expert_gate.shape[2]
+    any_spec = pl.BlockSpec(memory_space=pl.ANY)
+    vmem_spec = pl.BlockSpec(memory_space=pltpu.VMEM)
+    bf16, f32 = jnp.bfloat16, jnp.float32
+    dma = pltpu.SemaphoreType.DMA
+    routed = (layers, peers, cap, model_width)
+    chunks = (layers, tokens_here, model_width)
+    return pl.pallas_call(
+        functools.partial(moe_kernel, layers, peers, size_tp, cap, top_count),
+        out_shape=jax.ShapeDtypeStruct((tokens_here, model_width), bf16),
+        in_specs=[vmem_spec] * 3 + [any_spec] * 6,
+        out_specs=vmem_spec,
+        scratch_shapes=[
+            pltpu.VMEM(chunks, bf16),
+            pltpu.VMEM((layers, 2 * top_count, tokens_here), f32),
+            pltpu.VMEM(routed, bf16),
+            pltpu.VMEM(routed, bf16),
+            pltpu.VMEM(routed, bf16),
+            pltpu.VMEM(routed, bf16),
+            pltpu.VMEM(chunks, bf16),
+            pltpu.VMEM(chunks, bf16),
+            pltpu.VMEM((tokens_here, model_width), f32),
+            pltpu.VMEM((model_width, hidden_width), bf16),
+            pltpu.VMEM((model_width, hidden_width), bf16),
+            pltpu.VMEM((hidden_width, model_width), bf16),
+            pltpu.VMEM((model_width, expert_width), bf16),
+            pltpu.VMEM((model_width, expert_width), bf16),
+            pltpu.VMEM((expert_width, model_width), bf16),
+            dma((6,)),
+            dma((2,)),
+            dma((2, layers)),
+            dma((layers,)),
+            dma((layers,)),
+            dma((layers,)),
+            dma((layers, peers)),
+            dma((layers, peers)),
+            dma((layers, peers)),
+            dma((layers, peers)),
+            dma((layers,)),
+            dma((layers,)),
+        ],
+        compiler_params=pltpu.CompilerParams(
+            collective_id=0, has_side_effects=True, vmem_limit_bytes=58 * 1024 * 1024
+        ),
+    )(
+        normed,
+        settled,
+        meta,
+        shared_gate,
+        shared_up,
+        shared_down,
+        expert_gate,
+        expert_up,
+        expert_down,
     )
-    outgoing = normed[slot_token].reshape(capacity, experts, model_width)
-    arrived = lax.all_to_all(outgoing, ("sp", "tp"), split_axis=1, concat_axis=1, tiled=True)
-    item_total = arrived.shape[0]
-    flat_rows = arrived.reshape(item_total * experts, model_width)
-    expert_rows = swiglu(flat_rows, expert_gate[0], expert_up[0], expert_down[0]).astype(
-        jnp.bfloat16
-    )
-    results = expert_rows.reshape(item_total, experts, model_width)
-    returned = lax.all_to_all(results, ("sp", "tp"), split_axis=1, concat_axis=1, tiled=True)
-    picked = returned.reshape(capacity * experts, model_width)[slot_index].reshape(
-        tokens_here, top_count, model_width
-    )
-    weights = route_score / jnp.sum(route_score, axis=-1, keepdims=True) * routed_scale
-    routed = jnp.einsum("tk,tkd->td", weights, picked.astype(jnp.float32))
-    return (settled_wide + shared + routed).astype(jnp.bfloat16)
 
 
 def solution(mesh):

time: 226 us -> 141 us (0.62)
  the two profiles are of different devices: /device:TPU:0 before, /device:TPU:27 now
where the time goes in v1:
time: 141 us; the launch traced here: 140 us
  Pallas kernels  119 us (84%)
  local copies, waits for them, and re-layouts  6.16 us (4%)
  blocking collectives  4.54 us (3%)
  other arithmetic  3.76 us (3%)
  matrix products  3.59 us (3%)
  starting transfers between devices  3.11 us (2%)
    pallas_call x1, Pallas kernels, on_device(): pl.pallas_call(functools.partial(moe_kernel, layers, peers, size_tp, cap,...  119 us
    all_to_all x1, blocking collectives, on_device(): lax.all_to_all(mixed_rows, 'tp', split_axis=0, concat_axis=1, tiled=True)  4.54 us
    ppermute x1, starting transfers between devices, from_behind(): return lax.ppermute(shard, axis, pairs)  3.11 us
    dot_general x1, matrix products, on_device(): projected = jnp.dot(swapped, out_proj, preferred_element_type=jnp.float32)  3.04 us
    unnamed x12, local copies, waits for them, and re-layouts  3.03 us
  transfers between devices with their start and end apart: 1, of which 0 were waited for; matrix products, arithmetic and copies ran while one was open for 4% of the time, Pallas kernels for 0%

profile of v1, /device:TPU:27, one launch (start us, length us, event | category | flops | bytes accessed | tf_op | source)
XLA Modules:
  0.0 140.4 jit_solution(7908987930783273553)
XLA Ops:
  0.0 0.0 copy-start
  0.0 0.8 slice.118
  0.8 3.1 %collective-permute-start = (bf16[15,512]{1,0:T(8,128)(2,1)S(1)}, bf16[15,512]{1,0:T(8,128)(2,1)S(1)}, u32[]{:S(2)}, u32[]{:S(2)}) collective-permute-start(bf16[15,512]{1,0:T(8,128)(2,1)S(1)} %slice.118), channel_id=1, source_target_pairs={{0,2},{2,4},{4,6},{6,8},{8,10},{10,12},{12,14},{14,16},{16,18},{18... | collective-permute-start | bytes 46088 | tf_op jit(solution)/shard_map/ppermute | solution.py:19
  3.9 1.0 copy_bitcast_fusion
  4.9 0.8 copy.24
  5.7 0.1 eq.15
  5.8 0.3 fusion.1
  6.1 0.1 reduce_sum.31
  6.2 0.1 copy.25
  6.3 0.7 reduce_sum.32
  7.0 0.7 divide_multiply_fusion
  7.7 0.6 maximum_bitcast_fusion.meta_ref
  8.3 0.8 dynamic_slice.7
  9.1 0.0 collective-permute-done
  9.1 0.1 maximum_convert_fusion
  9.2 0.1 fusion.25
  9.2 0.0 copy-start.2
  9.4 0.1 fusion.10
  9.5 0.1 fusion.19
  9.6 0.1 fusion.13
  9.7 0.0 copy-start.3
  9.7 0.1 fusion.16
  9.8 0.0 copy-done
  9.8 0.3 copy-done.2
  10.2 0.3 convolution_bitcast_fusion
  10.5 0.3 reshape.84
  10.7 0.1 fusion.6
  10.9 4.5 %all_to_all.16 = bf16[2,128,512]{1,2,0:T(8,128)(2,1)S(1)} all-to-all(bf16[2,128,512]{1,2,0:T(8,128)(2,1)S(1)} %fusion.6), channel_id=1, replica_groups=mesh['sp'=16,'tp'=2] {'tp'}, dimensions={0} | all-to-all | bytes 524288 | tf_op jit(solution)/shard_map/all_to_all | solution.py:377
  15.4 0.0 copy-done.3
  15.4 0.0 copy-start.4
  15.4 3.0 %fusion.2 = (f32[128]{0:T(128)S(1)}, bf16[128,2048]{1,0:T(8,128)(2,1)S(1)}) fusion(bf16[128,1024]{0,1:T(8,128)(2,1)S(1)} %bitcast.54, bf16[1024,2048]{1,0:T(8,128)(2,1)} %param.18, bf16[128,2048]{1,0:T(8,128)(2,1)S(1)} %copy-done.3), kind=kOutput, calls=%fused_computation.7 | convolution fusion | flops 538443648 | bytes 5505536 | tf_op jit(solution)/shard_map/dot_general | solution.py:378
  18.5 0.0 copy-start.1
  18.5 0.0 copy-done.4
  18.5 1.0 fusion.4.normed_ref
  19.5 0.0 copy-done.1
  19.5 119.0 %shard_map.136 = bf16[128,2048]{1,0:T(8,128)(2,1)} custom-call(bf16[128,2048]{1,0:T(8,128)(2,1)} %fusion.4.normed_ref, bf16[128,2048]{1,0:T(8,128)(2,1)} %copy-done.1, f32[8,128]{1,0:T(8,128)} %maximum_bitcast_fusion.meta_ref, bf16[2048,512]{1,0:T(8,128)(2,1)} %sg_hbm.1, bf16[2048,512]{1,0:T(8,128)(2,1)} %su_hbm.1, bf16[512,2048]{1,0:T(8,128)(2,1)} %sd_hbm.1, ...), custom_call_target="tpu_custom_call" | custom-call | tf_op jit(solution)/shard_map/pallas_call | solution.py:410
  138.5 1.9 %copy.36 = bf16[128,2048]{1,0:T(8,128)(2,1)} copy(bf16[128,2048]{1,0:T(8,128)(2,1)} %shard_map.136) | data formatting | bytes 1048576
  (9 shorter events, 0.1 us)
Async XLA Ops:
  0.0 9.8 %copy-start = (bf16[8,128,128]{2,1,0:T(8,128)(2,1)S(1)}, bf16[8,128,128]{2,1,0:T(8,128)(2,1)}, u32[]{:S(2)}) copy-start(bf16[8,128,128]{2,1,0:T(8,128)(2,1)} %param.16) | copy-start | bytes 786436
  0.8 8.3 %collective-permute-start = (bf16[15,512]{1,0:T(8,128)(2,1)S(1)}, bf16[15,512]{1,0:T(8,128)(2,1)S(1)}, u32[]{:S(2)}, u32[]{:S(2)}) collective-permute-start(bf16[15,512]{1,0:T(8,128)(2,1)S(1)} %slice.118), channel_id=1, source_target_pairs={{0,2},{2,4},{4,6},{6,8},{8,10},{10,12},{12,14},{14,16},{16,18},{18... | collective-permute-start | bytes 46088 | tf_op jit(solution)/shard_map/ppermute | solution.py:19
  9.2 1.0 copy-start.2
  9.7 5.7 %copy-start.3 = (bf16[128,2048]{1,0:T(8,128)(2,1)S(1)}, bf16[128,2048]{1,0:T(8,128)(2,1)}, u32[]{:S(2)}) copy-start(bf16[128,2048]{1,0:T(8,128)(2,1)} %param.14) | copy-start | bytes 1572868
  15.4 3.1 %copy-start.4 = (f32[2048]{0:T(1024)S(1)}, f32[2048]{0:T(1024)}, u32[]{:S(2)}) copy-start(f32[2048]{0:T(1024)} %param.19) | copy-start | bytes 24580
  18.5 1.0 copy-start.1

commit v2 on v1

--- a/solution.py
+++ b/solution.py
@@ -110,6 +110,8 @@
     own_meta = pltpu.make_async_copy(meta_ref, metas.at[z], own_sem.at[1])
     own_rows.start()
     own_meta.start()
+    for load in loads:
+        load.start()
 
     barrier = pltpu.get_barrier_semaphore()
     for o in range(1, layers):
@@ -269,7 +271,7 @@
             part_copy(s, z).start()
 
     def shared():
-        for load in loads:
+        for load in loads[:3]:
             load.wait()
         hidden = mlp(normed_ref[...], sg, su)
         for col in range(0, width, step_cols):
@@ -278,28 +280,40 @@
                 jnp.float32
             )
 
+    at_end = near == 0
+
     def step(i, carry):
+        later = jnp.logical_and(i >= 3, at_end)
+
+        @pl.when(later)
+        def _():
+            combine(i - 2)
+
         @pl.when(i < layers)
         def _():
             dispatch(i)
 
-        @pl.when(i == 0)
-        def _():
-            shared()
-
-        @pl.when(jnp.logical_and(i >= 1, i <= layers))
+        @pl.when(i >= 2)
         def _():
             expert(i - 1)
 
-        @pl.when(i >= 2)
+        @pl.when(jnp.logical_and(i >= 3, jnp.logical_not(at_end)))
         def _():
             combine(i - 2)
 
         return carry
 
-    for load in loads:
-        load.start()
-    lax.fori_loop(0, layers + 2, step, 0)
+    def last(j, carry):
+        combine((layers - 1) * (1 - j))
+        return carry
+
+    dispatch(jnp.int32(0))
+    shared()
+    for load in loads[3:]:
+        load.wait()
+    lax.fori_loop(1, layers + 1, step, 0)
+    expert(jnp.int32(0))
+    lax.fori_loop(0, 2, last, 0)
 
     def drain(s, carry):
         @pl.when(goes_up(s))

time: 141 us -> 133 us (0.943)
  Pallas kernels: 119 us -> 111 us
    pallas_call x1, Pallas kernels: 119 us -> 111 us  [on_device(): pl.pallas_call(functools.partial(moe_kernel, layers, peers, size_tp, cap,...]
where the time goes in v2:
time: 133 us
  Pallas kernels  111 us (83%)
  local copies, waits for them, and re-layouts  6.16 us (5%)
  blocking collectives  4.54 us (3%)
  other arithmetic  3.76 us (3%)
  matrix products  3.59 us (3%)
  starting transfers between devices  3.11 us (2%)
    pallas_call x1, Pallas kernels, on_device(): pl.pallas_call(functools.partial(moe_kernel, layers, peers, size_tp, cap,...  111 us
    all_to_all x1, blocking collectives, on_device(): lax.all_to_all(mixed_rows, 'tp', split_axis=0, concat_axis=1, tiled=True)  4.54 us
    ppermute x1, starting transfers between devices, from_behind(): return lax.ppermute(shard, axis, pairs)  3.11 us
    dot_general x1, matrix products, on_device(): projected = jnp.dot(swapped, out_proj, preferred_element_type=jnp.float32)  3.04 us
    unnamed x12, local copies, waits for them, and re-layouts  3.03 us
  transfers between devices with their start and end apart: 1, of which 0 were waited for; matrix products, arithmetic and copies ran while one was open for 4% of the time, Pallas kernels for 0%

profile of v2, /device:TPU:27, one launch (start us, length us, event | category | flops | bytes accessed | tf_op | source)
XLA Modules:
  0.0 132.5 jit_solution(13863563167005872154)
XLA Ops:
  0.0 0.0 copy-start
  0.0 0.8 slice.118
  0.8 3.1 %collective-permute-start = (bf16[15,512]{1,0:T(8,128)(2,1)S(1)}, bf16[15,512]{1,0:T(8,128)(2,1)S(1)}, u32[]{:S(2)}, u32[]{:S(2)}) collective-permute-start(bf16[15,512]{1,0:T(8,128)(2,1)S(1)} %slice.118), channel_id=1, source_target_pairs={{0,2},{2,4},{4,6},{6,8},{8,10},{10,12},{12,14},{14,16},{16,18},{18... | collective-permute-start | bytes 46088 | tf_op jit(solution)/shard_map/ppermute | solution.py:19
  3.9 1.0 copy_bitcast_fusion
  4.9 0.8 copy.24
  5.7 0.1 eq.15
  5.8 0.3 fusion.1
  6.1 0.1 reduce_sum.31
  6.2 0.1 copy.25
  6.3 0.7 reduce_sum.32
  7.0 0.7 divide_multiply_fusion
  7.7 0.6 maximum_bitcast_fusion.meta_ref
  8.3 0.8 dynamic_slice.7
  9.1 0.0 collective-permute-done
  9.1 0.1 maximum_convert_fusion
  9.2 0.1 fusion.25
  9.2 0.0 copy-start.2
  9.4 0.1 fusion.10
  9.5 0.1 fusion.19
  9.6 0.1 fusion.13
  9.7 0.0 copy-start.3
  9.7 0.1 fusion.16
  9.8 0.0 copy-done
  9.8 0.3 copy-done.2
  10.2 0.3 convolution_bitcast_fusion
  10.5 0.3 reshape.84
  10.7 0.1 fusion.6
  10.9 4.5 %all_to_all.16 = bf16[2,128,512]{1,2,0:T(8,128)(2,1)S(1)} all-to-all(bf16[2,128,512]{1,2,0:T(8,128)(2,1)S(1)} %fusion.6), channel_id=1, replica_groups=mesh['sp'=16,'tp'=2] {'tp'}, dimensions={0} | all-to-all | bytes 524288 | tf_op jit(solution)/shard_map/all_to_all | solution.py:391
  15.4 0.0 copy-done.3
  15.4 0.0 copy-start.4
  15.4 3.0 %fusion.2 = (f32[128]{0:T(128)S(1)}, bf16[128,2048]{1,0:T(8,128)(2,1)S(1)}) fusion(bf16[128,1024]{0,1:T(8,128)(2,1)S(1)} %bitcast.54, bf16[1024,2048]{1,0:T(8,128)(2,1)} %param.18, bf16[128,2048]{1,0:T(8,128)(2,1)S(1)} %copy-done.3), kind=kOutput, calls=%fused_computation.7 | convolution fusion | flops 538443648 | bytes 5505536 | tf_op jit(solution)/shard_map/dot_general | solution.py:392
  18.5 0.0 copy-start.1
  18.5 0.0 copy-done.4
  18.5 1.0 fusion.4.normed_ref
  19.5 0.0 copy-done.1
  19.5 111.1 %shard_map.136 = bf16[128,2048]{1,0:T(8,128)(2,1)} custom-call(bf16[128,2048]{1,0:T(8,128)(2,1)} %fusion.4.normed_ref, bf16[128,2048]{1,0:T(8,128)(2,1)} %copy-done.1, f32[8,128]{1,0:T(8,128)} %maximum_bitcast_fusion.meta_ref, bf16[2048,512]{1,0:T(8,128)(2,1)} %sg_hbm.1, bf16[2048,512]{1,0:T(8,128)(2,1)} %su_hbm.1, bf16[512,2048]{1,0:T(8,128)(2,1)} %sd_hbm.1, ...), custom_call_target="tpu_custom_call" | custom-call | tf_op jit(solution)/shard_map/pallas_call | solution.py:424
  130.6 1.9 %copy.36 = bf16[128,2048]{1,0:T(8,128)(2,1)} copy(bf16[128,2048]{1,0:T(8,128)(2,1)} %shard_map.136) | data formatting | bytes 1048576
  (9 shorter events, 0.1 us)
Async XLA Ops:
  0.0 9.8 %copy-start = (bf16[8,128,128]{2,1,0:T(8,128)(2,1)S(1)}, bf16[8,128,128]{2,1,0:T(8,128)(2,1)}, u32[]{:S(2)}) copy-start(bf16[8,128,128]{2,1,0:T(8,128)(2,1)} %param.16) | copy-start | bytes 786436
  0.8 8.3 %collective-permute-start = (bf16[15,512]{1,0:T(8,128)(2,1)S(1)}, bf16[15,512]{1,0:T(8,128)(2,1)S(1)}, u32[]{:S(2)}, u32[]{:S(2)}) collective-permute-start(bf16[15,512]{1,0:T(8,128)(2,1)S(1)} %slice.118), channel_id=1, source_target_pairs={{0,2},{2,4},{4,6},{6,8},{8,10},{10,12},{12,14},{14,16},{16,18},{18... | collective-permute-start | bytes 46088 | tf_op jit(solution)/shard_map/ppermute | solution.py:19
  9.2 1.0 copy-start.2
  9.7 5.7 %copy-start.3 = (bf16[128,2048]{1,0:T(8,128)(2,1)S(1)}, bf16[128,2048]{1,0:T(8,128)(2,1)}, u32[]{:S(2)}) copy-start(bf16[128,2048]{1,0:T(8,128)(2,1)} %param.14) | copy-start | bytes 1572868
  15.4 3.1 %copy-start.4 = (f32[2048]{0:T(1024)S(1)}, f32[2048]{0:T(1024)}, u32[]{:S(2)}) copy-start(f32[2048]{0:T(1024)} %param.19) | copy-start | bytes 24580
  18.5 1.0 copy-start.1
